TPU v7x, 256 devices: a whole 4x4x8 slice. The times are simulated.
256 devices in a mesh: ep: 64 (over z, x, core), tp: 4 (over y).
Axes of the slice: x: 4, y: 4, z: 8, core: 2. Of those that a mesh axis runs over, the one named last changes fastest.
Arguments:
- tokens: bfloat16 [32768, 4096], P('ep', 'tp'), may hold values from -100 to 100, as said below
- routes: int32 [32768, 2], P('ep'), may hold values from 0 to 127, all different within a row; in each aligned block of 512 rows (0 to 511, 512 to 1023, ...) at most 16 rows name the same one
- route_weights: float32 [32768, 2], P('ep'), may hold values from 0.1 to 1
- norm_gain: float32 [4096], P('tp'), may hold values from 0.1 to 1.9
- gate_weight: bfloat16 [128, 4096, 512], P('ep', 'tp'), may hold values from -0.09375 to 0.09375
- up_weight: bfloat16 [128, 4096, 512], P('ep', 'tp'), may hold values from -0.09375 to 0.09375
- down_weight: bfloat16 [128, 512, 4096], P('ep', None, 'tp'), may hold values from -0.25 to 0.25
- final_gain: float32 [4096], P('tp'), may hold values from 0.1 to 1.9
Outputs:
- mixed: bfloat16 [32768, 4096], P('ep', 'tp')
Inputs may be any that keep to these rules, and one draw needn't show every extreme that they name: `tokens`: real-valued activations whose features differ in scale. `routes`: each row names 2 different experts; among the 512 rows of one aligned block no expert is named more than 16 times, a bound that some block reaches.
All inputs are finite; a program needn't handle non-finite values.
Results may differ from a plain program's by a relative error of at most 0.018.
Values may be sent and summed in bfloat16 or wider, within the bound.
No kernel may reach another device: no remote copies, remote signals or barrier semaphores. Data moves between devices by JAX's collectives and lax.ppermute only.
A program may use at most 64 MiB of HBM per device.

v0:
```python
import jax
import jax.numpy as jnp
from jax import lax
from jax.sharding import PartitionSpec as P

D = 4096


EPSILON = 1e-06


def in_blocks(x, dim, peers):
    before, after = (x.shape[:dim], x.shape[dim + 1 :])
    return jnp.moveaxis(x.reshape(*before, peers, -1, *after), dim, 0)


def sent_and_summed(x, axis, dim):
    peers = lax.axis_size(axis)
    tiles = lax.all_to_all(in_blocks(x, dim, peers), axis, 0, 0, tiled=True)
    return jnp.sum(tiles.astype(jnp.float32), axis=0)


def side_by_side(arrays, axis, dim, along):
    ends, at = ([], 0)
    for a in arrays[:-1]:
        at += a.shape[along]
        ends.append(at)
    both = jnp.concatenate(arrays, axis=along)
    return tuple(jnp.split(sent_and_summed(both, axis, dim), ends, axis=along))


def from_everyone(x, axis):
    copies = jnp.broadcast_to(x, (lax.axis_size(axis), *x.shape))
    return lax.all_to_all(copies, axis, split_axis=0, concat_axis=0, tiled=True)


def joined_along(tiles, dim):
    dims = list(tiles.shape[1:])
    dims[dim] *= tiles.shape[0]
    return jnp.moveaxis(tiles, 0, dim).reshape(dims)


def collect(x, axis, dim):
    tiles = from_everyone(x, axis)
    return joined_along(tiles, dim)


def taken_together(x, axis):
    everything = from_everyone(x, axis)
    return jnp.sum(everything, axis=0)


def expert_rows(weights, block):
    w_gate, w_up, w_down = weights
    gate = jnp.einsum("scd,df->scf", block, w_gate, preferred_element_type=jnp.float32)
    upper = jnp.einsum("scd,df->scf", block, w_up, preferred_element_type=jnp.float32)
    gate_sum, upper_sum = side_by_side(
        (gate.astype(jnp.bfloat16), upper.astype(jnp.bfloat16)), "tp", 2, 0
    )
    share = (jax.nn.silu(gate_sum) * upper_sum).astype(jnp.bfloat16)
    hidden = collect(share, "tp", 2)
    return jnp.einsum("scf,fd->scd", hidden, w_down, preferred_element_type=jnp.float32).astype(
        jnp.bfloat16
    )


def serve_all(weight_list, block):
    results = [
        expert_rows(weight_list[member], block[:, member]) for member in range(len(weight_list))
    ]
    return lax.all_to_all(jnp.stack(results, axis=1), "ep", split_axis=0, concat_axis=0, tiled=True)


def body(tokens, routes, route_weights, norm_gain, gate_weight, up_weight, down_weight, final_gain):
    ep_count = lax.axis_size("ep")
    local_count = gate_weight.shape[0]
    experts = ep_count * local_count
    tok_rows = tokens.shape[0]
    top_count = routes.shape[1]
    capacity = 4 * tok_rows // experts
    values = tokens.astype(jnp.float32)
    squares = taken_together(jnp.sum(values * values, axis=-1), "tp")
    normed = (values * lax.rsqrt(squares / D + EPSILON)[:, None] * norm_gain).astype(jnp.bfloat16)
    chosen = routes.reshape(-1)
    onehot = (chosen[:, None] == jnp.arange(experts, dtype=jnp.int32)[None, :]).astype(jnp.int32)
    slots = jnp.sum((jnp.cumsum(onehot, axis=0) - onehot) * onehot, axis=1)
    target = chosen * capacity + slots
    owners = jnp.arange(tok_rows * top_count, dtype=jnp.int32) // top_count
    table = jnp.full((experts * capacity,), tok_rows, jnp.int32).at[target].set(owners)
    padded = jnp.concatenate([normed, jnp.zeros((1, normed.shape[1]), jnp.bfloat16)], axis=0)
    outgoing = padded[table].reshape(ep_count, local_count, capacity, normed.shape[1])
    weight_list = [
        (gate_weight[member], up_weight[member], down_weight[member])
        for member in range(local_count)
    ]
    arrived = serve_all(
        weight_list, lax.all_to_all(outgoing, "ep", split_axis=0, concat_axis=0, tiled=True)
    )
    returned = arrived.reshape(experts * capacity, normed.shape[1])
    position = target.reshape(tok_rows, top_count)
    combined = jnp.zeros((tok_rows, normed.shape[1]), jnp.float32)
    for which in range(top_count):
        combined = combined + route_weights[:, which : which + 1] * returned[
            position[:, which]
        ].astype(jnp.float32)
    closing = taken_together(jnp.sum(combined * combined, axis=-1), "tp")
    return (combined * lax.rsqrt(closing / D + EPSILON)[:, None] * final_gain).astype(jnp.bfloat16)


def solution(mesh):
    in_specs = (
        P("ep", "tp"),
        P("ep", None),
        P("ep", None),
        P("tp"),
        P("ep", "tp", None),
        P("ep", "tp", None),
        P("ep", None, "tp"),
        P("tp"),
    )
    out_specs = P("ep", "tp")
    return jax.shard_map(body, mesh=mesh, in_specs=in_specs, out_specs=out_specs, check_vma=False)
```

profile of v0, /device:TPU:2, one launch (start us, length us, event | category | flops | bytes accessed | tf_op | source)
XLA Modules:
  0.0 366.8 jit_solution(13011418187434321295)
XLA Ops:
  0.0 1.5 fusion
  2.1 4.5 %all-to-all-start = ((f32[4,1,512]{2,1,0:T(1,128)}), f32[4,1,512]{2,1,0:T(1,128)S(1)}, u32[]{:S(2)}, u32[]{:S(2)}) async-start(f32[4,1,512]{2,1,0:T(1,128)} %broadcast_in_dim.12), calls=%async_computation | async-start | bytes 16384 | tf_op jit(solution)/shard_map/all_to_all | solution.py:34
  9.1 4.3 %scatter_custom_fusion = s32[2048]{0:T(1024)S(1)} fusion(s32[1024]{0:T(1024)S(1)} %bitcast.101, s32[1024]{0:T(1024)S(1)} %add_select_fusion, s32[]{:T(128)} %constant.39.clone.1), kind=kCustom, calls=%fused_computation.77 | custom fusion | bytes 8196 | tf_op jit(solution)/shard_map/scatter | solution.py:89
  13.9 9.7 %gather_fusion = bf16[2048,1024]{1,0:T(8,128)(2,1)} fusion(bf16[513,1024]{1,0:T(8,128)(2,1)S(1)} %concatenate.9, s32[2048]{0:T(1024)S(1)} %fusion.36), kind=kCustom, calls=%fused_computation | custom fusion | bytes 8396800 | tf_op jit(solution)/shard_map/gather | solution.py:91
  23.6 108.3 %all_to_all.42 = bf16[64,2,16,1024]{3,2,1,0:T(8,128)(2,1)S(1)} all-to-all(bf16[64,2,16,1024]{3,2,1,0:T(8,128)(2,1)} %bitcast.95), channel_id=1, replica_groups=mesh['ep'=64,'tp'=4] {'ep'}, dimensions={0} | all-to-all | bytes 8388608 | tf_op jit(solution)/shard_map/all_to_all | solution.py:97
  131.9 1.2 fusion.10
  134.0 1.0 copy-done.7
  135.0 1.2 fusion.9
  136.2 1.7 bitcast_bitcast_fusion.1
  137.9 4.8 %all-to-all-start.2 = ((bf16[4,128,16,128]{3,2,1,0:T(8,128)(2,1)}), bf16[4,128,16,128]{3,2,1,0:T(8,128)(2,1)S(1)}, u32[]{:S(2)}, u32[]{:S(2)}) async-start(bf16[4,128,16,128]{3,2,1,0:T(8,128)(2,1)} %bitcast_bitcast_fusion.1), calls=%async_computation.2 | async-start | bytes 4194304 | tf_op jit(solution)/shard_map/all_to_all | solution.py:19
  142.7 3.2 fusion.8
  146.6 1.2 fusion.7
  147.8 1.7 bitcast_bitcast_fusion
  149.5 18.0 %all-to-all-done.2 = bf16[4,128,16,128]{3,2,1,0:T(8,128)(2,1)S(1)} async-done(((bf16[4,128,16,128]{3,2,1,0:T(8,128)(2,1)}), bf16[4,128,16,128]{3,2,1,0:T(8,128)(2,1)S(1)}, u32[]{:S(2)}, u32[]{:S(2)}) %all-to-all-start.2) | async-done | bytes 2097184 | tf_op jit(solution)/shard_map/all_to_all | solution.py:19
  167.6 4.4 %all-to-all-start.4 = ((bf16[4,128,16,128]{3,2,1,0:T(8,128)(2,1)}), bf16[4,128,16,128]{3,2,1,0:T(8,128)(2,1)}, u32[]{:S(2)}, u32[]{:S(2)}) async-start(bf16[4,128,16,128]{3,2,1,0:T(8,128)(2,1)} %bitcast_bitcast_fusion), calls=%async_computation.4 | async-start | bytes 4194304 | tf_op jit(solution)/shard_map/all_to_all | solution.py:19
  172.5 23.5 %all-to-all-done.4 = bf16[4,128,16,128]{3,2,1,0:T(8,128)(2,1)} async-done(((bf16[4,128,16,128]{3,2,1,0:T(8,128)(2,1)}), bf16[4,128,16,128]{3,2,1,0:T(8,128)(2,1)}, u32[]{:S(2)}, u32[]{:S(2)}) %all-to-all-start.4) | async-done | bytes 2097184 | tf_op jit(solution)/shard_map/all_to_all | solution.py:19
  196.0 1.1 broadcast_in_dim.30
  197.1 3.5 all-to-all-start.3
  200.6 2.0 convert_reduce_fusion
  202.8 9.6 %all-to-all-done.3 = bf16[4,64,16,128]{3,2,1,0:T(8,128)(2,1)S(1)} async-done(((bf16[4,64,16,128]{3,2,1,0:T(8,128)(2,1)}), bf16[4,64,16,128]{3,2,1,0:T(8,128)(2,1)S(1)}, u32[]{:S(2)}, u32[]{:S(2)}) %all-to-all-start.3) | async-done | bytes 1048608 | tf_op jit(solution)/shard_map/all_to_all | solution.py:34
  212.5 1.1 broadcast_in_dim.31
  213.6 4.4 %all-to-all-start.5 = ((bf16[4,64,16,128]{3,2,1,0:T(8,128)(2,1)}), bf16[4,64,16,128]{3,2,1,0:T(8,128)(2,1)}, u32[]{:S(2)}, u32[]{:S(2)}) async-start(bf16[4,64,16,128]{3,2,1,0:T(8,128)(2,1)} %broadcast_in_dim.31), calls=%async_computation.5 | async-start | bytes 2097152 | tf_op jit(solution)/shard_map/all_to_all | solution.py:34
  218.0 2.5 convert_bitcast_fusion.1
  220.5 8.3 %all-to-all-done.5 = bf16[4,64,16,128]{3,2,1,0:T(8,128)(2,1)} async-done(((bf16[4,64,16,128]{3,2,1,0:T(8,128)(2,1)}), bf16[4,64,16,128]{3,2,1,0:T(8,128)(2,1)}, u32[]{:S(2)}, u32[]{:S(2)}) %all-to-all-start.5) | async-done | bytes 1048608 | tf_op jit(solution)/shard_map/all_to_all | solution.py:34
  228.8 2.8 convert_bitcast_fusion
  232.0 2.4 copy.59
  234.4 15.4 %all-to-all-start.6 = ((bf16[64,2,16,1024]{3,2,1,0:T(8,128)(2,1)}), bf16[64,2,16,1024]{3,2,1,0:T(8,128)(2,1)}, u32[]{:S(2)}, u32[]{:S(2)}) async-start(bf16[64,2,16,1024]{3,2,1,0:T(8,128)(2,1)} %copy.59), calls=%async_computation.6 | async-start | bytes 8388608 | tf_op jit(solution)/shard_map/all_to_all | solution.py:71
  250.2 95.8 %all-to-all-done.6 = bf16[64,2,16,1024]{3,2,1,0:T(8,128)(2,1)} async-done(((bf16[64,2,16,1024]{3,2,1,0:T(8,128)(2,1)}), bf16[64,2,16,1024]{3,2,1,0:T(8,128)(2,1)}, u32[]{:S(2)}, u32[]{:S(2)}) %all-to-all-start.6) | async-done | bytes 4194336 | tf_op jit(solution)/shard_map/all_to_all | solution.py:71
  345.9 5.5 %gather_fusion.2 = bf16[512,1024]{1,0:T(8,128)(2,1)S(1)} fusion(bf16[2048,1024]{1,0:T(8,128)(2,1)} %bitcast.27, s32[1024]{0:T(1024)S(1)} %get-tuple-element.11), kind=kCustom, calls=%fused_computation.2 | custom fusion | bytes 2099200 | tf_op jit(solution)/shard_map/gather | solution.py:103
  351.4 5.5 %gather_fusion.1 = bf16[512,1024]{1,0:T(8,128)(2,1)S(1)} fusion(bf16[2048,1024]{1,0:T(8,128)(2,1)} %bitcast.27, s32[1024]{0:T(1024)S(1)} %get-tuple-element.12), kind=kCustom, calls=%fused_computation.1 | custom fusion | bytes 2099200 | tf_op jit(solution)/shard_map/gather | solution.py:103
  357.5 7.7 %all_to_all.43 = f32[4,1,512]{2,1,0:T(1,128)S(1)} all-to-all(f32[4,1,512]{2,1,0:T(1,128)S(1)} %broadcast_in_dim.32), channel_id=1, replica_groups=mesh['ep'=64,'tp'=4] {'tp'}, dimensions={0} | all-to-all | bytes 16384 | tf_op jit(solution)/shard_map/all_to_all | solution.py:34
  365.2 1.6 multiply_convert_fusion
  (51 shorter events, 6.9 us)
Async XLA Ops:
  2.1 11.3 %all-to-all-start = ((f32[4,1,512]{2,1,0:T(1,128)}), f32[4,1,512]{2,1,0:T(1,128)S(1)}, u32[]{:S(2)}, u32[]{:S(2)}) async-start(f32[4,1,512]{2,1,0:T(1,128)} %broadcast_in_dim.12), calls=%async_computation | async-start | bytes 16384 | tf_op jit(solution)/shard_map/all_to_all | solution.py:34
  8.1 5.4 %copy-start = (bf16[512,1024]{1,0:T(8,128)(2,1)S(1)}, bf16[512,1024]{1,0:T(8,128)(2,1)}, u32[]{:S(2)}) copy-start(bf16[512,1024]{1,0:T(8,128)(2,1)} %param.8) | copy-start | bytes 3145732
  8.1 5.4 %copy-start.3 = (f32[1024]{0:T(1024)S(1)}, f32[1024]{0:T(1024)}, u32[]{:S(2)}) copy-start(f32[1024]{0:T(1024)} %param.11) | copy-start | bytes 12292
  23.6 108.3 %copy-start.6 = (bf16[2,1024,512]{2,1,0:T(8,128)(2,1)S(1)}, bf16[2,1024,512]{2,1,0:T(8,128)(2,1)}, u32[]{:S(2)}) copy-start(bf16[2,1024,512]{2,1,0:T(8,128)(2,1)} %param.13) | copy-start | bytes 6291460
  131.9 2.1 copy-start.1
  131.9 3.1 copy-start.7
  137.9 29.6 %all-to-all-start.2 = ((bf16[4,128,16,128]{3,2,1,0:T(8,128)(2,1)}), bf16[4,128,16,128]{3,2,1,0:T(8,128)(2,1)S(1)}, u32[]{:S(2)}, u32[]{:S(2)}) async-start(bf16[4,128,16,128]{3,2,1,0:T(8,128)(2,1)} %bitcast_bitcast_fusion.1), calls=%async_computation.2 | async-start | bytes 4194304 | tf_op jit(solution)/shard_map/all_to_all | solution.py:19
  142.7 3.3 copy-start.2
  142.7 3.8 %copy-start.8 = (bf16[2,1024,512]{2,1,0:T(8,128)(2,1)S(1)}, bf16[2,1024,512]{2,1,0:T(8,128)(2,1)}, u32[]{:S(2)}) copy-start(bf16[2,1024,512]{2,1,0:T(8,128)(2,1)} %param.12) | copy-start | bytes 6291460
  167.6 28.5 %all-to-all-start.4 = ((bf16[4,128,16,128]{3,2,1,0:T(8,128)(2,1)}), bf16[4,128,16,128]{3,2,1,0:T(8,128)(2,1)}, u32[]{:S(2)}, u32[]{:S(2)}) async-start(bf16[4,128,16,128]{3,2,1,0:T(8,128)(2,1)} %bitcast_bitcast_fusion), calls=%async_computation.4 | async-start | bytes 4194304 | tf_op jit(solution)/shard_map/all_to_all | solution.py:19
  197.1 15.3 %all-to-all-start.3 = ((bf16[4,64,16,128]{3,2,1,0:T(8,128)(2,1)}), bf16[4,64,16,128]{3,2,1,0:T(8,128)(2,1)S(1)}, u32[]{:S(2)}, u32[]{:S(2)}) async-start(bf16[4,64,16,128]{3,2,1,0:T(8,128)(2,1)} %broadcast_in_dim.30), calls=%async_computation.3 | async-start | bytes 2097152 | tf_op jit(solution)/shard_map/all_to_all | solution.py:34
  213.6 15.2 %all-to-all-start.5 = ((bf16[4,64,16,128]{3,2,1,0:T(8,128)(2,1)}), bf16[4,64,16,128]{3,2,1,0:T(8,128)(2,1)}, u32[]{:S(2)}, u32[]{:S(2)}) async-start(bf16[4,64,16,128]{3,2,1,0:T(8,128)(2,1)} %broadcast_in_dim.31), calls=%async_computation.5 | async-start | bytes 2097152 | tf_op jit(solution)/shard_map/all_to_all | solution.py:34
  234.4 15.8 %copy-start.5 = (f32[512,2]{0,1:T(2,128)S(1)}, f32[512,2]{0,1:T(2,128)}, u32[]{:S(2)}) copy-start(f32[512,2]{0,1:T(2,128)} %param.10) | copy-start | bytes 12292
  234.4 111.5 %all-to-all-start.6 = ((bf16[64,2,16,1024]{3,2,1,0:T(8,128)(2,1)}), bf16[64,2,16,1024]{3,2,1,0:T(8,128)(2,1)}, u32[]{:S(2)}, u32[]{:S(2)}) async-start(bf16[64,2,16,1024]{3,2,1,0:T(8,128)(2,1)} %copy.59), calls=%async_computation.6 | async-start | bytes 8388608 | tf_op jit(solution)/shard_map/all_to_all | solution.py:71
  356.9 8.4 %copy-start.4 = (f32[1024]{0:T(1024)S(1)}, f32[1024]{0:T(1024)}, u32[]{:S(2)}) copy-start(f32[1024]{0:T(1024)} %param.15) | copy-start | bytes 12292
where the time goes:
time: 368 us; the launch traced here: 367 us
  waiting for transfers between devices  155 us (42%)
  blocking collectives  116 us (32%)
  starting transfers between devices  37.1 us (10%)
  local copies, waits for them, and re-layouts  34.4 us (9%)
  matrix products  12.2 us (3%)
  other arithmetic  11.5 us (3%)
    all_to_all x1, blocking collectives, body(): lax.all_to_all(outgoing, 'ep', split_axis=0, concat_axis=0, tiled=True)  108 us
    all_to_all x1, waiting for transfers between devices, serve_all(): lax.all_to_all(jnp.stack(results, axis=1), 'ep', split_axis=0, concat_axi...  95.8 us
    all_to_all x2, waiting for transfers between devices, sent_and_summed(): tiles = lax.all_to_all(in_blocks(x, dim, peers), axis, 0, 0, tiled=True)  41.6 us
    all_to_all x3, waiting for transfers between devices, from_everyone(): return lax.all_to_all(copies, axis, split_axis=0, concat_axis=0, tiled=True)  17.9 us
    all_to_all x1, starting transfers between devices, serve_all(): lax.all_to_all(jnp.stack(results, axis=1), 'ep', split_axis=0, concat_axi...  15.4 us
    all_to_all x3, starting transfers between devices, from_everyone(): return lax.all_to_all(copies, axis, split_axis=0, concat_axis=0, tiled=True)  12.4 us
    gather x2, local copies, waits for them, and re-layouts, body(): returned[position[:, which]].astype(jnp.float32)  10.9 us
    gather x1, local copies, waits for them, and re-layouts, body(): padded[table].reshape(ep_count, local_count, capacity, normed.shape[1])  9.67 us
  transfers between devices with their start and end apart: 6, of which 5 were waited for; matrix products, arithmetic and copies ran while one was open for 5% of the time, Pallas kernels for 0%

commit v1 on v0

v1 whole, which is shorter than its diff:
```python
import jax
import jax.numpy as jnp
from jax import lax
from jax.sharding import PartitionSpec as P

D = 4096
EPSILON = 1e-06
CHUNKS = 2
F32 = jnp.float32
BF16 = jnp.bfloat16


def shifted(x, axis, by):
    n = lax.axis_size(axis)
    return lax.ppermute(x, axis, [(i, (i + by) % n) for i in range(n)])


def total_over(x, axis):
    parts = [shifted(x, axis, by) for by in range(1, lax.axis_size(axis))]
    for part in parts:
        x = x + part
    return x


def block(x, at, width, dim):
    return lax.dynamic_slice_in_dim(x, at * width, width, dim)


def reduce_scattered(x, axis):
    n = lax.axis_size(axis)
    me = lax.axis_index(axis)
    width = x.shape[1] // n
    acc = block(x, me, width, 1).astype(F32)
    for by in range(1, n):
        acc = acc + shifted(block(x, (me + by) % n, width, 1), axis, by).astype(F32)
    return acc


def gathered(x, axis):
    return [x] + [shifted(x, axis, by) for by in range(1, lax.axis_size(axis))]


def positions(routes, experts):
    rows = routes.shape[0]
    ids = lax.broadcasted_iota(jnp.int32, (experts, rows), 0)
    named = [ids == routes[:, k][None, :] for k in range(routes.shape[1])]
    either = sum(n.astype(BF16) for n in named)
    earlier = (
        lax.broadcasted_iota(jnp.int32, (rows, rows), 0)
        < lax.broadcasted_iota(jnp.int32, (rows, rows), 1)
    ).astype(BF16)
    before = jnp.dot(either, earlier, preferred_element_type=F32)
    return [jnp.sum(jnp.where(n, before, 0.0), axis=0).astype(jnp.int32) for n in named]


def body(tokens, routes, route_weights, norm_gain, gate_weight, up_weight, down_weight, final_gain):
    ep = lax.axis_size("ep")
    members = gate_weight.shape[0]
    experts = ep * members
    rows, width = tokens.shape
    top = routes.shape[1]
    capacity = 4 * rows // experts
    part = capacity // CHUNKS
    values = tokens.astype(F32)
    squares = total_over(jnp.sum(values * values, axis=-1)[None, :], "tp")[0]
    slots = positions(routes, experts)
    normed = (values * lax.rsqrt(squares / D + EPSILON)[:, None] * norm_gain).astype(BF16)
    chunk_rows = experts * part
    ids = lax.broadcasted_iota(jnp.int32, (chunk_rows, rows), 0)

    def placed(c):
        out = []
        for k in range(top):
            inside = (slots[k] >= c * part) & (slots[k] < (c + 1) * part)
            at = jnp.where(inside, routes[:, k] * part + slots[k] - c * part, chunk_rows)
            out.append(ids == at[None, :])
        return out

    def sent(c):
        pick = sum(p.astype(BF16) for p in placed(c))
        rows_out = jnp.dot(pick, normed, preferred_element_type=F32).astype(BF16)
        return lax.all_to_all(
            rows_out.reshape(ep, members * part, width), "ep", 0, 0, tiled=True
        )

    def served(arrived):
        arrived = arrived.reshape(ep, members, part, width)
        hidden_dim = gate_weight.shape[2]
        tp = lax.axis_size("tp")
        partial = []
        for m in range(members):
            r = arrived[:, m].reshape(ep * part, width)
            g = jnp.dot(r, gate_weight[m], preferred_element_type=F32).astype(BF16)
            u = jnp.dot(r, up_weight[m], preferred_element_type=F32).astype(BF16)
            partial.append(jnp.stack([g, u], axis=0))
        both = jnp.stack(partial, axis=0)
        w = hidden_dim // tp
        me = lax.axis_index("tp")
        acc = block(both, me, w, 3).astype(F32)
        for by in range(1, tp):
            acc = acc + shifted(block(both, (me + by) % tp, w, 3), "tp", by).astype(F32)
        share = (jax.nn.silu(acc[:, 0]) * acc[:, 1]).astype(BF16)
        total = 0.0
        for by, piece in enumerate(gathered(share, "tp")):
            wd = block(down_weight, (me - by) % tp, w, 1)
            total = total + jnp.einsum("mrf,mfd->mrd", piece, wd, preferred_element_type=F32)
        out = total.astype(BF16).reshape(members, ep, part, width)
        return jnp.moveaxis(out, 0, 1).reshape(ep, members * part, width)

    arrived = [sent(c) for c in range(CHUNKS)]
    combined = jnp.zeros((rows, width), F32)
    for c in range(CHUNKS):
        back = lax.all_to_all(served(arrived[c]), "ep", 0, 0, tiled=True)
        back = back.reshape(chunk_rows, width)
        weights = sum(
            jnp.where(p, route_weights[:, k][None, :], 0.0) for k, p in enumerate(placed(c))
        )
        high = weights.astype(BF16)
        low = (weights - high.astype(F32)).astype(BF16)
        for w in (high, low):
            combined = combined + lax.dot_general(
                w, back, (((0,), (0,)), ((), ())), preferred_element_type=F32
            )
    closing = total_over(jnp.sum(combined * combined, axis=-1)[None, :], "tp")[0]
    return (combined * lax.rsqrt(closing / D + EPSILON)[:, None] * final_gain).astype(BF16)


def solution(mesh):
    in_specs = (
        P("ep", "tp"),
        P("ep", None),
        P("ep", None),
        P("tp"),
        P("ep", "tp", None),
        P("ep", "tp", None),
        P("ep", None, "tp"),
        P("tp"),
    )
    return jax.shard_map(
        body, mesh=mesh, in_specs=in_specs, out_specs=P("ep", "tp"), check_vma=False
    )
```

time: 368 us -> 283 us (0.77)
  blocking collectives: 116 us -> 0 us
  matrix products: 12.2 us -> 43.1 us
  local copies, waits for them, and re-layouts: 34.4 us -> 5 us
  starting transfers between devices: 37.1 us -> 62.3 us
  waiting for transfers between devices: 155 us -> 165 us
  other arithmetic: 11.5 us -> 7.06 us
    all_to_all x2 -> x0, blocking collectives: 116 us -> none  [the longest x1 108 us: body(): lax.all_to_all(outgoing, 'ep', split_axis=0, concat_axis=0, tiled=True)]
    ppermute x0 -> x18, waiting for transfers between devices: none -> 73.8 us  [shifted(): return lax.ppermute(x, axis, [(i, (i + by) % n) for i in range(n)])]
    all_to_all x6 -> x4, waiting for transfers between devices: 155 us -> 90.9 us  [the longest x2 48.3 us: sent(): lax.all_to_all(rows_out.reshape(ep, members * part, width), 'ep', 0, 0, t...]
    dot_general x6 -> x23, matrix products: 12.2 us -> 43.1 us  [the longest x4 14.7 us: body(): lax.dot_general(w, back, (((0,), (0,)), ((), ())), preferred_element_type...]
    ppermute x0 -> x18, starting transfers between devices: none -> 23.4 us  [shifted(): return lax.ppermute(x, axis, [(i, (i + by) % n) for i in range(n)])]
    gather x3 -> x0, local copies, waits for them, and re-layouts: 20.6 us -> none  [the longest x2 10.9 us: body(): returned[position[:, which]].astype(jnp.float32)]
    scatter x1 -> x0, local copies, waits for them, and re-layouts: 4.32 us -> none  [body(): jnp.full((experts * capacity,), tok_rows, jnp.int32).at[target].set(owners)]
    all_to_all x6 -> x4, starting transfers between devices: 37.1 us -> 38.9 us  [the longest x2 21.1 us: body(): back = lax.all_to_all(served(arrived[c]), 'ep', 0, 0, tiled=True)]
  transfers between devices with their start and end apart: 6 -> 22, of which waited for: 5 -> 14; matrix products, arithmetic and copies ran while one was open for 5% -> 15% of each run, Pallas kernels for 0% -> 0%
where the time goes in v1:
time: 283 us
  waiting for transfers between devices  165 us (58%)
  starting transfers between devices  62.3 us (22%)
  matrix products  43.1 us (15%)
  other arithmetic  7.06 us (2%)
  local copies, waits for them, and re-layouts  5 us (2%)
    ppermute x18, waiting for transfers between devices, shifted(): return lax.ppermute(x, axis, [(i, (i + by) % n) for i in range(n)])  73.8 us
    all_to_all x2, waiting for transfers between devices, sent(): lax.all_to_all(rows_out.reshape(ep, members * part, width), 'ep', 0, 0, t...  48.3 us
    all_to_all x2, waiting for transfers between devices, body(): back = lax.all_to_all(served(arrived[c]), 'ep', 0, 0, tiled=True)  42.6 us
    ppermute x18, starting transfers between devices, shifted(): return lax.ppermute(x, axis, [(i, (i + by) % n) for i in range(n)])  23.4 us
    all_to_all x2, starting transfers between devices, body(): back = lax.all_to_all(served(arrived[c]), 'ep', 0, 0, tiled=True)  21.1 us
    all_to_all x2, starting transfers between devices, sent(): lax.all_to_all(rows_out.reshape(ep, members * part, width), 'ep', 0, 0, t...  17.8 us
    dot_general x4, matrix products, body(): lax.dot_general(w, back, (((0,), (0,)), ((), ())), preferred_element_type...  14.7 us
    dot_general x4, matrix products, served(): g = jnp.dot(r, gate_weight[m], preferred_element_type=F32).astype(BF16)  8.66 us
  transfers between devices with their start and end apart: 22, of which 14 were waited for; matrix products, arithmetic and copies ran while one was open for 15% of the time, Pallas kernels for 0%

profile of v1, /device:TPU:2, one launch (start us, length us, event | category | flops | bytes accessed | tf_op | source)
XLA Modules:
  0.0 282.5 jit_solution(2964075030835109459)
XLA Ops:
  3.3 2.9 %collective-permute-start.1 = (f32[1,512]{1,0:T(1,128)S(1)}, f32[1,512]{1,0:T(1,128)S(1)}, u32[]{:S(2)}, u32[]{:S(2)}) collective-permute-start(f32[1,512]{1,0:T(1,128)S(1)} %bitcast.127), channel_id=1, source_target_pairs={{0,2},{1,3},{2,0},{3,1},{4,6},{5,7},{6,4},{7,5},{8,10},{9,11},{10,... | collective-permute-start | bytes 6152 | tf_op jit(solution)/shard_map/ppermute | solution.py:15
  9.8 2.8 %convolution_convert_fusion.1 = bf16[1024,1024]{1,0:T(8,128)(2,1)} fusion(s32[512]{0:T(512)S(1)} %get-tuple-element.24, s32[512]{0:T(512)S(1)} %get-tuple-element.13, bf16[512,1024]{1,0:T(8,128)(2,1)S(1)} %copy-done.2, f32[1024]{0:T(1024)S(1)} %copy-done.9, f32[512]{0:T(512)S(1)} %bitcast.135), kind=kOutput, calls=%fused_computation.45 | convolution fusion | flops 1081081856 | bytes 3155968 | tf_op jit(solution)/shard_map/dot_general | solution.py:81
  12.7 12.2 %all-to-all-start = ((bf16[64,16,1024]{2,1,0:T(8,128)(2,1)}), bf16[64,16,1024]{2,1,0:T(8,128)(2,1)}, u32[]{:S(2)}, u32[]{:S(2)}) async-start(bf16[64,16,1024]{2,1,0:T(8,128)(2,1)} %bitcast.125), calls=%async_computation | async-start | bytes 4194304 | tf_op jit(solution)/shard_map/all_to_all | solution.py:82
  24.9 2.8 convolution_convert_fusion
  27.7 48.3 %all-to-all-done = bf16[64,16,1024]{2,1,0:T(8,128)(2,1)} async-done(((bf16[64,16,1024]{2,1,0:T(8,128)(2,1)}), bf16[64,16,1024]{2,1,0:T(8,128)(2,1)}, u32[]{:S(2)}, u32[]{:S(2)}) %all-to-all-start) | async-done | bytes 2097184 | tf_op jit(solution)/shard_map/all_to_all | solution.py:82
  76.0 5.6 %all-to-all-start.2 = ((bf16[64,16,1024]{2,1,0:T(8,128)(2,1)}), bf16[64,16,1024]{2,1,0:T(8,128)(2,1)}, u32[]{:S(2)}, u32[]{:S(2)}) async-start(bf16[64,16,1024]{2,1,0:T(8,128)(2,1)} %bitcast.124), calls=%async_computation.2 | async-start | bytes 4194304 | tf_op jit(solution)/shard_map/all_to_all | solution.py:82
  81.7 2.4 fusion.11
  84.1 2.1 fusion.12
  86.3 1.9 fusion.13
  92.7 3.8 %collective-permute-start.4 = (bf16[2,2,512,128]{3,2,1,0:T(8,128)(2,1)}, bf16[2,2,512,128]{3,2,1,0:T(8,128)(2,1)}, u32[]{:S(2)}, u32[]{:S(2)}) collective-permute-start(bf16[2,2,512,128]{3,2,1,0:T(8,128)(2,1)} %get-tuple-element.8), channel_id=1, source_target_pairs={{0,2},{1,3},{2,0},{3,1},{4,6},{5,7},{6,4},{7,5},{8,10},{9,11},{10,... | collective-permute-start | bytes 1572872 | tf_op jit(solution)/shard_map/ppermute | solution.py:15
  96.7 11.4 %collective-permute-done.3 = bf16[2,2,512,128]{3,2,1,0:T(8,128)(2,1)} collective-permute-done((bf16[2,2,512,128]{3,2,1,0:T(8,128)(2,1)}, bf16[2,2,512,128]{3,2,1,0:T(8,128)(2,1)}, u32[]{:S(2)}, u32[]{:S(2)}) %collective-permute-start.3) | collective-permute-done | bytes 524320 | tf_op jit(solution)/shard_map/ppermute | solution.py:15
  108.1 12.0 %collective-permute-done.4 = bf16[2,2,512,128]{3,2,1,0:T(8,128)(2,1)} collective-permute-done((bf16[2,2,512,128]{3,2,1,0:T(8,128)(2,1)}, bf16[2,2,512,128]{3,2,1,0:T(8,128)(2,1)}, u32[]{:S(2)}, u32[]{:S(2)}) %collective-permute-start.4) | collective-permute-done | bytes 524320 | tf_op jit(solution)/shard_map/ppermute | solution.py:15
  122.8 3.2 %collective-permute-start.7 = (bf16[2,512,128]{2,1,0:T(8,128)(2,1)S(1)}, bf16[2,512,128]{2,1,0:T(8,128)(2,1)S(1)}, u32[]{:S(2)}, u32[]{:S(2)}) collective-permute-start(bf16[2,512,128]{2,1,0:T(8,128)(2,1)S(1)} %fusion.74), channel_id=1, source_target_pairs={{0,2},{1,3},{2,0},{3,1},{4,6},{5,7},{6,4},{7,5},{8,10},{9,11},{10,... | collective-permute-start | bytes 786440 | tf_op jit(solution)/shard_map/ppermute | solution.py:15
  126.8 4.3 %collective-permute-done.6 = bf16[2,512,128]{2,1,0:T(8,128)(2,1)S(1)} collective-permute-done((bf16[2,512,128]{2,1,0:T(8,128)(2,1)S(1)}, bf16[2,512,128]{2,1,0:T(8,128)(2,1)S(1)}, u32[]{:S(2)}, u32[]{:S(2)}) %collective-permute-start.6) | collective-permute-done | bytes 262176 | tf_op jit(solution)/shard_map/ppermute | solution.py:15
  131.8 6.1 %collective-permute-done.7 = bf16[2,512,128]{2,1,0:T(8,128)(2,1)S(1)} collective-permute-done((bf16[2,512,128]{2,1,0:T(8,128)(2,1)S(1)}, bf16[2,512,128]{2,1,0:T(8,128)(2,1)S(1)}, u32[]{:S(2)}, u32[]{:S(2)}) %collective-permute-start.7) | collective-permute-done | bytes 262176 | tf_op jit(solution)/shard_map/ppermute | solution.py:15
  141.0 10.5 %all-to-all-start.1 = ((bf16[64,16,1024]{2,1,0:T(8,128)(2,1)}), bf16[64,16,1024]{2,1,0:T(8,128)(2,1)}, u32[]{:S(2)}, u32[]{:S(2)}) async-start(bf16[64,16,1024]{2,1,0:T(8,128)(2,1)} %bitcast.122), calls=%async_computation.1 | async-start | bytes 4194304 | tf_op jit(solution)/shard_map/all_to_all | solution.py:113
  151.5 2.4 fusion.17
  153.9 2.1 fusion.18
  156.1 1.9 fusion.15
  158.1 1.9 fusion.16
  160.9 2.0 collective-permute-start.11
  162.9 14.0 %collective-permute-done.10 = bf16[2,2,512,128]{3,2,0,1:T(8,128)(2,1)S(1)} collective-permute-done((bf16[2,2,512,128]{3,2,0,1:T(8,128)(2,1)S(1)}, bf16[2,2,512,128]{3,2,0,1:T(8,128)(2,1)S(1)}, u32[]{:S(2)}, u32[]{:S(2)}) %collective-permute-start.10) | collective-permute-done | bytes 524320 | tf_op jit(solution)/shard_map/ppermute | solution.py:15
  176.9 9.2 %collective-permute-done.11 = bf16[2,2,512,128]{3,2,0,1:T(8,128)(2,1)S(1)} collective-permute-done((bf16[2,2,512,128]{3,2,0,1:T(8,128)(2,1)S(1)}, bf16[2,2,512,128]{3,2,0,1:T(8,128)(2,1)S(1)}, u32[]{:S(2)}, u32[]{:S(2)}) %collective-permute-start.11) | collective-permute-done | bytes 524320 | tf_op jit(solution)/shard_map/ppermute | solution.py:15
  187.7 2.9 %collective-permute-start.13 = (bf16[2,512,128]{2,1,0:T(8,128)(2,1)S(1)}, bf16[2,512,128]{2,1,0:T(8,128)(2,1)S(1)}, u32[]{:S(2)}, u32[]{:S(2)}) collective-permute-start(bf16[2,512,128]{2,1,0:T(8,128)(2,1)S(1)} %fusion.72), channel_id=1, source_target_pairs={{0,2},{1,3},{2,0},{3,1},{4,6},{5,7},{6,4},{7,5},{8,10},{9,11},{10,... | collective-permute-start | bytes 786440 | tf_op jit(solution)/shard_map/ppermute | solution.py:15
  191.6 11.2 %collective-permute-done.12 = bf16[2,512,128]{2,1,0:T(8,128)(2,1)S(1)} collective-permute-done((bf16[2,512,128]{2,1,0:T(8,128)(2,1)S(1)}, bf16[2,512,128]{2,1,0:T(8,128)(2,1)S(1)}, u32[]{:S(2)}, u32[]{:S(2)}) %collective-permute-start.12) | collective-permute-done | bytes 262176 | tf_op jit(solution)/shard_map/ppermute | solution.py:15
  206.7 10.6 %all-to-all-start.3 = ((bf16[64,16,1024]{2,1,0:T(8,128)(2,1)}), bf16[64,16,1024]{2,1,0:T(8,128)(2,1)}, u32[]{:S(2)}, u32[]{:S(2)}) async-start(bf16[64,16,1024]{2,1,0:T(8,128)(2,1)} %bitcast.123), calls=%async_computation.3 | async-start | bytes 4194304 | tf_op jit(solution)/shard_map/all_to_all | solution.py:113
  217.3 4.3 %fusion.50 = f32[512,1024]{1,0:T(8,128)} fusion(bf16[1024,1024]{1,0:T(8,128)(2,1)} %bitcast.25, f32[512]{0:T(512)S(1)} %bitcast.145, s32[512]{0:T(512)S(1)} %get-tuple-element.24, f32[512]{0:T(512)S(1)} %bitcast.141, s32[512]{0:T(512)S(1)} %get-tuple-element.13), kind=kOutput, calls=%fused_computation.99 | convolution fusion | flops 1076887552 | bytes 4202496 | tf_op jit(solution)/shard_map/dot_general | solution.py:121
  221.6 4.3 %fusion.22 = f32[512,1024]{1,0:T(8,128)} fusion(bf16[1024,1024]{1,0:T(8,128)(2,1)} %bitcast.25, f32[512]{0:T(512)S(1)} %bitcast.146, s32[512]{0:T(512)S(1)} %get-tuple-element.24, f32[512]{0:T(512)S(1)} %bitcast.142, s32[512]{0:T(512)S(1)} %get-tuple-element.13), kind=kOutput, calls=%fused_computation.63 | convolution fusion | flops 1078460416 | bytes 4202496 | tf_op jit(solution)/shard_map/dot_general | solution.py:121
  225.9 42.6 %all-to-all-done.3 = bf16[64,16,1024]{2,1,0:T(8,128)(2,1)} async-done(((bf16[64,16,1024]{2,1,0:T(8,128)(2,1)}), bf16[64,16,1024]{2,1,0:T(8,128)(2,1)}, u32[]{:S(2)}, u32[]{:S(2)}) %all-to-all-start.3) | async-done | bytes 2097184 | tf_op jit(solution)/shard_map/all_to_all | solution.py:113
  268.4 3.0 %fusion.53 = f32[512,1024]{1,0:T(8,128)S(1)} fusion(bf16[1024,1024]{1,0:T(8,128)(2,1)} %bitcast.41, s32[512]{0:T(512)S(1)} %get-tuple-element.23, s32[512]{0:T(512)S(1)} %get-tuple-element.14, f32[512]{0:T(512)S(1)} %bitcast.147, f32[512]{0:T(512)S(1)} %bitcast.143), kind=kOutput, calls=%fused_computation.100 | convolution fusion | flops 1076887552 | bytes 4202496 | tf_op jit(solution)/shard_map/dot_general | solution.py:121
  271.5 3.1 %multiply_reduce_fusion = (f32[512]{0:T(512)S(1)}, f32[512,1024]{1,0:T(8,128)S(1)}) fusion(bf16[1024,1024]{1,0:T(8,128)(2,1)} %bitcast.41, s32[512]{0:T(512)S(1)} %get-tuple-element.23, s32[512]{0:T(512)S(1)} %get-tuple-element.14, f32[512]{0:T(512)S(1)} %bitcast.148, f32[512]{0:T(512)S(1)} %bitcast.144, f32[512,1024]{1,0:T(8,128)S(1)} %fusion.53, ...), kind=kOutput, calls=%fused_computation.28 | convolution fusion | flops 1081081344 | bytes 10496000 | tf_op jit(solution)/shard_map/dot_general | solution.py:121
  274.7 3.0 %collective-permute-start.16 = (f32[1,512]{1,0:T(1,128)S(1)}, f32[1,512]{1,0:T(1,128)S(1)}, u32[]{:S(2)}, u32[]{:S(2)}) collective-permute-start(f32[1,512]{1,0:T(1,128)S(1)} %bitcast.138), channel_id=1, source_target_pairs={{0,2},{1,3},{2,0},{3,1},{4,6},{5,7},{6,4},{7,5},{8,10},{9,11},{10,... | collective-permute-start | bytes 6152 | tf_op jit(solution)/shard_map/ppermute | solution.py:15
  (78 shorter events, 31.1 us)
Async XLA Ops:
  0.0 126.1 %copy-start = (bf16[2,512,1024]{2,1,0:T(8,128)(2,1)S(1)}, bf16[2,512,1024]{2,1,0:T(8,128)(2,1)}, u32[]{:S(2)}) copy-start(bf16[2,512,1024]{2,1,0:T(8,128)(2,1)} %param.14) | copy-start | bytes 6291460
  0.0 9.8 %copy-start.2 = (bf16[512,1024]{1,0:T(8,128)(2,1)S(1)}, bf16[512,1024]{1,0:T(8,128)(2,1)}, u32[]{:S(2)}) copy-start(bf16[512,1024]{1,0:T(8,128)(2,1)} %param.8) | copy-start | bytes 3145732
  0.0 9.8 %copy-start.9 = (f32[1024]{0:T(1024)S(1)}, f32[1024]{0:T(1024)}, u32[]{:S(2)}) copy-start(f32[1024]{0:T(1024)} %param.11) | copy-start | bytes 12292
  1.7 7.0 %collective-permute-start = (f32[1,512]{1,0:T(1,128)S(1)}, f32[1,512]{1,0:T(1,128)S(1)}, u32[]{:S(2)}, u32[]{:S(2)}) collective-permute-start(f32[1,512]{1,0:T(1,128)S(1)} %bitcast.126), channel_id=1, source_target_pairs={{0,1},{1,2},{2,3},{3,0},{4,5},{5,6},{6,7},{7,4},{8,9},{9,10},{10,1... | collective-permute-start | bytes 6152 | tf_op jit(solution)/shard_map/ppermute | solution.py:15
  3.3 5.3 %collective-permute-start.1 = (f32[1,512]{1,0:T(1,128)S(1)}, f32[1,512]{1,0:T(1,128)S(1)}, u32[]{:S(2)}, u32[]{:S(2)}) collective-permute-start(f32[1,512]{1,0:T(1,128)S(1)} %bitcast.127), channel_id=1, source_target_pairs={{0,2},{1,3},{2,0},{3,1},{4,6},{5,7},{6,4},{7,5},{8,10},{9,11},{10,... | collective-permute-start | bytes 6152 | tf_op jit(solution)/shard_map/ppermute | solution.py:15
  6.2 3.6 %collective-permute-start.2 = (f32[1,512]{1,0:T(1,128)S(1)}, f32[1,512]{1,0:T(1,128)S(1)}, u32[]{:S(2)}, u32[]{:S(2)}) collective-permute-start(f32[1,512]{1,0:T(1,128)S(1)} %bitcast.128), channel_id=1, source_target_pairs={{0,3},{1,0},{2,1},{3,2},{4,7},{5,4},{6,5},{7,6},{8,11},{9,8},{10,9... | collective-permute-start | bytes 6152 | tf_op jit(solution)/shard_map/ppermute | solution.py:15
  12.7 63.4 %all-to-all-start = ((bf16[64,16,1024]{2,1,0:T(8,128)(2,1)}), bf16[64,16,1024]{2,1,0:T(8,128)(2,1)}, u32[]{:S(2)}, u32[]{:S(2)}) async-start(bf16[64,16,1024]{2,1,0:T(8,128)(2,1)} %bitcast.125), calls=%async_computation | async-start | bytes 4194304 | tf_op jit(solution)/shard_map/all_to_all | solution.py:82
  76.0 64.9 %all-to-all-start.2 = ((bf16[64,16,1024]{2,1,0:T(8,128)(2,1)}), bf16[64,16,1024]{2,1,0:T(8,128)(2,1)}, u32[]{:S(2)}, u32[]{:S(2)}) async-start(bf16[64,16,1024]{2,1,0:T(8,128)(2,1)} %bitcast.124), calls=%async_computation.2 | async-start | bytes 4194304 | tf_op jit(solution)/shard_map/all_to_all | solution.py:82
  81.7 2.4 copy-start.7
  92.5 15.5 %collective-permute-start.3 = (bf16[2,2,512,128]{3,2,1,0:T(8,128)(2,1)}, bf16[2,2,512,128]{3,2,1,0:T(8,128)(2,1)}, u32[]{:S(2)}, u32[]{:S(2)}) collective-permute-start(bf16[2,2,512,128]{3,2,1,0:T(8,128)(2,1)} %get-tuple-element.7), channel_id=1, source_target_pairs={{0,1},{1,2},{2,3},{3,0},{4,5},{5,6},{6,7},{7,4},{8,9},{9,10},{10,1... | collective-permute-start | bytes 1572872 | tf_op jit(solution)/shard_map/ppermute | solution.py:15
  92.7 27.3 %collective-permute-start.4 = (bf16[2,2,512,128]{3,2,1,0:T(8,128)(2,1)}, bf16[2,2,512,128]{3,2,1,0:T(8,128)(2,1)}, u32[]{:S(2)}, u32[]{:S(2)}) collective-permute-start(bf16[2,2,512,128]{3,2,1,0:T(8,128)(2,1)} %get-tuple-element.8), channel_id=1, source_target_pairs={{0,2},{1,3},{2,0},{3,1},{4,6},{5,7},{6,4},{7,5},{8,10},{9,11},{10,... | collective-permute-start | bytes 1572872 | tf_op jit(solution)/shard_map/ppermute | solution.py:15
  96.5 23.5 %collective-permute-start.5 = (bf16[2,2,512,128]{3,2,1,0:T(8,128)(2,1)}, bf16[2,2,512,128]{3,2,1,0:T(8,128)(2,1)}, u32[]{:S(2)}, u32[]{:S(2)}) collective-permute-start(bf16[2,2,512,128]{3,2,1,0:T(8,128)(2,1)} %get-tuple-element.9), channel_id=1, source_target_pairs={{0,3},{1,0},{2,1},{3,2},{4,7},{5,4},{6,5},{7,6},{8,11},{9,8},{10,9... | collective-permute-start | bytes 1572872 | tf_op jit(solution)/shard_map/ppermute | solution.py:15
  121.8 9.2 %collective-permute-start.6 = (bf16[2,512,128]{2,1,0:T(8,128)(2,1)S(1)}, bf16[2,512,128]{2,1,0:T(8,128)(2,1)S(1)}, u32[]{:S(2)}, u32[]{:S(2)}) collective-permute-start(bf16[2,512,128]{2,1,0:T(8,128)(2,1)S(1)} %fusion.74), channel_id=1, source_target_pairs={{0,1},{1,2},{2,3},{3,0},{4,5},{5,6},{6,7},{7,4},{8,9},{9,10},{10,1... | collective-permute-start | bytes 786440 | tf_op jit(solution)/shard_map/ppermute | solution.py:15
  122.8 15.1 %collective-permute-start.7 = (bf16[2,512,128]{2,1,0:T(8,128)(2,1)S(1)}, bf16[2,512,128]{2,1,0:T(8,128)(2,1)S(1)}, u32[]{:S(2)}, u32[]{:S(2)}) collective-permute-start(bf16[2,512,128]{2,1,0:T(8,128)(2,1)S(1)} %fusion.74), channel_id=1, source_target_pairs={{0,2},{1,3},{2,0},{3,1},{4,6},{5,7},{6,4},{7,5},{8,10},{9,11},{10,... | collective-permute-start | bytes 786440 | tf_op jit(solution)/shard_map/ppermute | solution.py:15
  126.0 12.5 %collective-permute-start.8 = (bf16[2,512,128]{2,1,0:T(8,128)(2,1)S(1)}, bf16[2,512,128]{2,1,0:T(8,128)(2,1)S(1)}, u32[]{:S(2)}, u32[]{:S(2)}) collective-permute-start(bf16[2,512,128]{2,1,0:T(8,128)(2,1)S(1)} %fusion.74), channel_id=1, source_target_pairs={{0,3},{1,0},{2,1},{3,2},{4,7},{5,4},{6,5},{7,6},{8,11},{9,8},{10,9... | collective-permute-start | bytes 786440 | tf_op jit(solution)/shard_map/ppermute | solution.py:15
  141.0 65.7 %all-to-all-start.1 = ((bf16[64,16,1024]{2,1,0:T(8,128)(2,1)}), bf16[64,16,1024]{2,1,0:T(8,128)(2,1)}, u32[]{:S(2)}, u32[]{:S(2)}) async-start(bf16[64,16,1024]{2,1,0:T(8,128)(2,1)} %bitcast.122), calls=%async_computation.1 | async-start | bytes 4194304 | tf_op jit(solution)/shard_map/all_to_all | solution.py:113
  151.5 2.4 copy-start.8
  153.9 2.2 copy-start.6
  160.4 16.4 %collective-permute-start.10 = (bf16[2,2,512,128]{3,2,0,1:T(8,128)(2,1)S(1)}, bf16[2,2,512,128]{3,2,0,1:T(8,128)(2,1)S(1)}, u32[]{:S(2)}, u32[]{:S(2)}) collective-permute-start(bf16[2,2,512,128]{3,2,0,1:T(8,128)(2,1)S(1)} %get-tuple-element.11), channel_id=1, source_target_pairs={{0,2},{1,3},{2,0},{3,1},{4,6},{5,7},{6,4},{7,5},{8,10},{9,11},{10,... | collective-permute-start | bytes 1572872 | tf_op jit(solution)/shard_map/ppermute | solution.py:15
  160.9 25.2 %collective-permute-start.11 = (bf16[2,2,512,128]{3,2,0,1:T(8,128)(2,1)S(1)}, bf16[2,2,512,128]{3,2,0,1:T(8,128)(2,1)S(1)}, u32[]{:S(2)}, u32[]{:S(2)}) collective-permute-start(bf16[2,2,512,128]{3,2,0,1:T(8,128)(2,1)S(1)} %get-tuple-element.12), channel_id=1, source_target_pairs={{0,3},{1,0},{2,1},{3,2},{4,7},{5,4},{6,5},{7,6},{8,11},{9,8},{10,9... | collective-permute-start | bytes 1572872 | tf_op jit(solution)/shard_map/ppermute | solution.py:15
  162.9 24.3 %collective-permute-start.9 = (bf16[2,2,512,128]{3,2,0,1:T(8,128)(2,1)S(1)}, bf16[2,2,512,128]{3,2,0,1:T(8,128)(2,1)S(1)}, u32[]{:S(2)}, u32[]{:S(2)}) collective-permute-start(bf16[2,2,512,128]{3,2,0,1:T(8,128)(2,1)S(1)} %get-tuple-element.10), channel_id=1, source_target_pairs={{0,1},{1,2},{2,3},{3,0},{4,5},{5,6},{6,7},{7,4},{8,9},{9,10},{10,1... | collective-permute-start | bytes 1572872 | tf_op jit(solution)/shard_map/ppermute | solution.py:15
  187.6 15.2 %collective-permute-start.12 = (bf16[2,512,128]{2,1,0:T(8,128)(2,1)S(1)}, bf16[2,512,128]{2,1,0:T(8,128)(2,1)S(1)}, u32[]{:S(2)}, u32[]{:S(2)}) collective-permute-start(bf16[2,512,128]{2,1,0:T(8,128)(2,1)S(1)} %fusion.72), channel_id=1, source_target_pairs={{0,1},{1,2},{2,3},{3,0},{4,5},{5,6},{6,7},{7,4},{8,9},{9,10},{10,1... | collective-permute-start | bytes 786440 | tf_op jit(solution)/shard_map/ppermute | solution.py:15
  187.7 15.8 %collective-permute-start.13 = (bf16[2,512,128]{2,1,0:T(8,128)(2,1)S(1)}, bf16[2,512,128]{2,1,0:T(8,128)(2,1)S(1)}, u32[]{:S(2)}, u32[]{:S(2)}) collective-permute-start(bf16[2,512,128]{2,1,0:T(8,128)(2,1)S(1)} %fusion.72), channel_id=1, source_target_pairs={{0,2},{1,3},{2,0},{3,1},{4,6},{5,7},{6,4},{7,5},{8,10},{9,11},{10,... | collective-permute-start | bytes 786440 | tf_op jit(solution)/shard_map/ppermute | solution.py:15
  190.7 13.6 %collective-permute-start.14 = (bf16[2,512,128]{2,1,0:T(8,128)(2,1)S(1)}, bf16[2,512,128]{2,1,0:T(8,128)(2,1)S(1)}, u32[]{:S(2)}, u32[]{:S(2)}) collective-permute-start(bf16[2,512,128]{2,1,0:T(8,128)(2,1)S(1)} %fusion.72), channel_id=1, source_target_pairs={{0,3},{1,0},{2,1},{3,2},{4,7},{5,4},{6,5},{7,6},{8,11},{9,8},{10,9... | collective-permute-start | bytes 786440 | tf_op jit(solution)/shard_map/ppermute | solution.py:15
  206.7 10.6 %copy-start.4 = (f32[512,2]{0,1:T(2,128)S(1)}, f32[512,2]{0,1:T(2,128)}, u32[]{:S(2)}) copy-start(f32[512,2]{0,1:T(2,128)} %param.10) | copy-start | bytes 12292
  206.7 61.8 %all-to-all-start.3 = ((bf16[64,16,1024]{2,1,0:T(8,128)(2,1)}), bf16[64,16,1024]{2,1,0:T(8,128)(2,1)}, u32[]{:S(2)}, u32[]{:S(2)}) async-start(bf16[64,16,1024]{2,1,0:T(8,128)(2,1)} %bitcast.123), calls=%async_computation.3 | async-start | bytes 4194304 | tf_op jit(solution)/shard_map/all_to_all | solution.py:113
  268.4 3.0 %copy-start.10 = (f32[512,1024]{1,0:T(8,128)S(1)}, f32[512,1024]{1,0:T(8,128)}, u32[]{:S(2)}) copy-start(f32[512,1024]{1,0:T(8,128)} %fusion.50) | copy-start | bytes 6291460
  268.4 3.1 %copy-start.11 = (f32[512,1024]{1,0:T(8,128)S(1)}, f32[512,1024]{1,0:T(8,128)}, u32[]{:S(2)}) copy-start(f32[512,1024]{1,0:T(8,128)} %fusion.22) | copy-start | bytes 6291460
  271.5 9.8 %copy-start.3 = (f32[1024]{0:T(1024)S(1)}, f32[1024]{0:T(1024)}, u32[]{:S(2)}) copy-start(f32[1024]{0:T(1024)} %param.15) | copy-start | bytes 12292
  274.6 4.9 %collective-permute-start.15 = (f32[1,512]{1,0:T(1,128)S(1)}, f32[1,512]{1,0:T(1,128)S(1)}, u32[]{:S(2)}, u32[]{:S(2)}) collective-permute-start(f32[1,512]{1,0:T(1,128)S(1)} %bitcast.137), channel_id=1, source_target_pairs={{0,1},{1,2},{2,3},{3,0},{4,5},{5,6},{6,7},{7,4},{8,9},{9,10},{10,1... | collective-permute-start | bytes 6152 | tf_op jit(solution)/shard_map/ppermute | solution.py:15
  274.7 5.2 %collective-permute-start.16 = (f32[1,512]{1,0:T(1,128)S(1)}, f32[1,512]{1,0:T(1,128)S(1)}, u32[]{:S(2)}, u32[]{:S(2)}) collective-permute-start(f32[1,512]{1,0:T(1,128)S(1)} %bitcast.138), channel_id=1, source_target_pairs={{0,2},{1,3},{2,0},{3,1},{4,6},{5,7},{6,4},{7,5},{8,10},{9,11},{10,... | collective-permute-start | bytes 6152 | tf_op jit(solution)/shard_map/ppermute | solution.py:15
  277.7 3.6 %collective-permute-start.17 = (f32[1,512]{1,0:T(1,128)S(1)}, f32[1,512]{1,0:T(1,128)S(1)}, u32[]{:S(2)}, u32[]{:S(2)}) collective-permute-start(f32[1,512]{1,0:T(1,128)S(1)} %bitcast.139), channel_id=1, source_target_pairs={{0,3},{1,0},{2,1},{3,2},{4,7},{5,4},{6,5},{7,6},{8,11},{9,8},{10,9... | collective-permute-start | bytes 6152 | tf_op jit(solution)/shard_map/ppermute | solution.py:15
  (2 other events, 3.2 us)
